TPU v7x, 32 devices: a whole 2x2x4 slice. The times are simulated.
32 devices in a mesh: sp: 8 (over z, y), tp: 4 (over x, core).
Axes of the slice: x: 2, y: 2, z: 4, core: 2. Of those that a mesh axis runs over, the one named last changes fastest.
Arguments:
- residual_in: bfloat16 [4096, 2048], P('sp'), may hold values from -6 to 6
- queries_nope: bfloat16 [4096, 1024], P('sp', 'tp'), may hold values from -15 to 15
- queries_rope: bfloat16 [4096, 512], P('sp', 'tp'), may hold values from -400 to 400
- latents: bfloat16 [4096, 256], P('sp'), may hold values from -6 to 6
- rope_keys: bfloat16 [4096, 32], P('sp'), may hold values from -8 to 8
- latent_norm_gain: float32 [256], replicated, may hold values from 0.1 to 1.9
- key_up_weight: bfloat16 [256, 1024], P(None, 'tp'), may hold values from -0.375 to 0.375
- value_up_weight: bfloat16 [256, 1024], P(None, 'tp'), may hold values from -0.375 to 0.375
- w_out: bfloat16 [1024, 2048], P('tp'), may hold values from -0.59765625 to 0.59765625
- norm_gain: float32 [2048], replicated, may hold values from 0.1 to 1.9
- w_up: bfloat16 [2048, 8192], P('sp', 'tp'), may hold values from -0.125 to 0.125
- w_down: bfloat16 [8192, 2048], P('tp', 'sp'), may hold values from -0.0625 to 0.0625
Outputs:
- layer_out: bfloat16 [4096, 2048], P('sp', 'tp')
All inputs are finite; a program needn't handle non-finite values.
Results may differ from a plain program's by a relative error of at most 0.015.
Values may be sent and summed in bfloat16 or wider, within the bound.
A program may use at most 128 MiB of HBM per device.

v0:
```python
import functools
import math

import jax
import jax.numpy as jnp
from jax import lax
from jax.experimental import pallas as pl
from jax.experimental.pallas import tpu as pltpu
from jax.sharding import PartitionSpec as P

UNROTATED_WIDTH = 64
ROPE = 32
LANES = 128
CHUNKS = 4

rope_base = 10000.0
epsilon = 1e-06
F32 = jnp.float32
BF16 = jnp.bfloat16
MESH = pl.DeviceIdType.MESH
NT = (((1,), (1,)), ((), ()))


def rotate(vectors, phases):
    half_width = vectors.shape[-1] // 2
    first_half = vectors[..., :half_width]
    second_half = vectors[..., half_width:]
    cosine = jnp.cos(phases)
    sine = jnp.sin(phases)
    return jnp.concatenate(
        [first_half * cosine - second_half * sine, second_half * cosine + first_half * sine],
        axis=-1,
    )


def rope_phases(positions, width):
    inverse = 1.0 / rope_base ** (jnp.arange(0, width, 2, dtype=jnp.float32) / width)
    return positions.astype(jnp.float32)[:, None] * inverse[None, :]


def rms_scale(vectors, gain_vec):
    return (
        vectors
        * lax.rsqrt(jnp.mean(vectors * vectors, axis=-1, keepdims=True) + epsilon)
        * gain_vec
    )


def ring_of(index, n):
    return index // 2 + (index % 2) * (n - 1 - 2 * (index // 2))


def index_of(place, n):
    return 2 * place + (place // (n // 2)) * (2 * n - 1 - 4 * place)


def ring_ids(n):
    place = ring_of(lax.axis_index("sp"), n)

    def at(offset):
        return index_of((place + offset + 2 * n) % n, n)

    return at


def attention_kernel(
    n, n_tp, heads, scale, q_ref, x_ref, wk_in, wv_in, wo_ref, wu_ref,
    part_ref, full_ref,
    wk_ref, wv_ref, xs, peak, acc, xsend, xrecv, ssend, srecv, wsend, wrecv, own_sem,
):
    at = ring_ids(n)
    tp = lax.axis_index("tp")
    me = lax.axis_index("sp")
    to = ((at(1), tp), (at(-1), tp))
    peers = [(tp + k) % n_tp for k in range(1, n_tp)]
    onward = (at(1 - 2 * (tp % 2)), tp)
    barrier = pltpu.get_barrier_semaphore()
    for target in list(to) + [(me, p) for p in peers]:
        pl.semaphore_signal(barrier, inc=1, device_id=target, device_id_type=MESH)
    pl.semaphore_wait(barrier, 2 + n_tp - 1)

    latent = wk_ref.shape[1]
    value_width = wv_ref.shape[0] // heads

    def x_copy(step, src):
        return pltpu.make_async_remote_copy(
            src_ref=src, dst_ref=xs.at[step + 1, tp],
            send_sem=xsend.at[step], recv_sem=xrecv.at[step],
            device_id=onward, device_id_type=MESH,
        )

    def share(step, k):
        return pltpu.make_async_remote_copy(
            src_ref=xs.at[step, tp], dst_ref=xs.at[step, tp],
            send_sem=ssend.at[step, k], recv_sem=srecv.at[step, k],
            device_id=(me, peers[k]), device_id_type=MESH,
        )

    def share_wait(step):
        for k in range(n_tp - 1):
            pltpu.make_async_remote_copy(
                src_ref=xs.at[step, tp], dst_ref=xs.at[step, (tp + n_tp - 1 - k) % n_tp],
                send_sem=ssend.at[step, k], recv_sem=srecv.at[step, k],
                device_id=(me, peers[k]), device_id_type=MESH,
            ).wait_recv()

    def w_copy(step, half, c, first):
        owner = at(-step) if half == 0 else at(step)
        return pltpu.make_async_remote_copy(
            src_ref=wu_ref.at[half, c] if first else full_ref.at[owner, half, c],
            dst_ref=full_ref.at[owner, half, c],
            send_sem=wsend.at[step, half, c], recv_sem=wrecv.at[step, half, c],
            device_id=to[half], device_id_type=MESH,
        )

    x_copy(0, x_ref.at[tp]).start()
    for c in range(CHUNKS):
        for half in range(2):
            w_copy(0, half, c, True).start()
    own = pltpu.make_async_copy(wu_ref, full_ref.at[me], own_sem)
    own.start()
    wk_ref[...] = jnp.transpose(wk_in[...].astype(F32)).astype(BF16)
    wv_ref[...] = jnp.transpose(wv_in[...].astype(F32)).astype(BF16)
    peak[...] = jnp.full(peak.shape, -1e30, F32)
    acc[...] = jnp.zeros(acc.shape, F32)

    def attend(blocks):
        block = jnp.concatenate(blocks, axis=1)
        lat = block[:latent]
        rot = block[latent:]
        keys = block.shape[1]
        k_all = jnp.dot(wk_ref[...], lat, preferred_element_type=F32).astype(BF16)
        v_all = jnp.dot(wv_ref[...], lat, preferred_element_type=F32).astype(BF16)
        k_pad = jnp.zeros((LANES - UNROTATED_WIDTH - rot.shape[0], keys), BF16)
        ones = jnp.ones((16, keys), BF16)
        v_pad = jnp.zeros((LANES - value_width - 16, keys), BF16)
        for h in range(heads):
            k_h = jnp.concatenate(
                [k_all[h * UNROTATED_WIDTH:(h + 1) * UNROTATED_WIDTH], rot, k_pad], axis=0)
            v_h = jnp.concatenate(
                [v_all[h * value_width:(h + 1) * value_width], ones, v_pad], axis=0)
            s = jnp.dot(q_ref[:, h * LANES:(h + 1) * LANES], k_h, preferred_element_type=F32)
            old = peak[h]
            new = jnp.maximum(old, jnp.max(s, axis=1, keepdims=True))
            p = jnp.exp2((s - new) * scale).astype(BF16)
            acc[h] = acc[h] * jnp.exp2((old - new) * scale) + lax.dot_general(
                p, v_h, NT, preferred_element_type=F32)
            peak[h] = new

    def turn(i, carry):
        x_copy(i - 1, x_ref.at[tp]).wait_recv()
        x_copy(i, xs.at[i, tp]).start()
        for k in range(n_tp - 1):
            share(i, k).start()
        for c in range(CHUNKS):
            for half in range(2):
                w_copy(i - 1, half, c, True).wait_recv()
                w_copy(i, half, c, False).start()

        @pl.when(i > 1)
        def _():
            share_wait(i - 1)
            attend([xs[i - 1, t] for t in range(n_tp)])

        return carry

    attend([x_ref[t] for t in range(n_tp)])
    lax.fori_loop(1, n - 1, turn, 0)
    x_copy(n - 2, x_ref.at[tp]).wait_recv()
    for k in range(n_tp - 1):
        share(n - 1, k).start()

    def last(i, carry):
        share_wait(i)
        attend([xs[i, t] for t in range(n_tp)])
        return carry

    lax.fori_loop(n - 2, n, last, 0)

    width = part_ref.shape[2]
    group = []
    for h in range(heads):
        a = acc[h]
        group.append((a[:, :value_width] / a[:, value_width:value_width + 1]).astype(BF16))
    attended = jnp.concatenate(group, axis=1)
    for j in range(part_ref.shape[0]):
        part_ref[j] = jnp.dot(
            attended, wo_ref[:, j * width:(j + 1) * width], preferred_element_type=F32
        ).astype(BF16)

    own.wait()
    for c in range(CHUNKS):
        for half in range(2):
            w_copy(n - 2, half, c, True).wait_recv()

    def drain(i, carry):
        x_copy(i, x_ref.at[tp]).wait_send()
        for k in range(n_tp - 1):
            share(i + 1, k).wait_send()
        for c in range(CHUNKS):
            for half in range(2):
                w_copy(i, half, c, True).wait_send()
        return carry

    lax.fori_loop(0, n - 1, drain, 0)


def feed_kernel(
    n, n_tp, narrow, part_ref, res_hbm, gain_ref, up_hbm, wd_hbm,
    out_ref,
    res_ref, up, down, parts, ys, sq, own_stream, hidden, pieces, fin,
    dsend, drecv, psend, precv, ysend, yrecv, qsend, qrecv, fsend, frecv, local,
):
    at = ring_ids(n)
    tp = lax.axis_index("tp")
    sp = lax.axis_index("sp")
    to = ((at(1), tp), (at(-1), tp))
    peers = [(tp + k) % n_tp for k in range(1, n_tp)]
    barrier = pltpu.get_barrier_semaphore()
    for target in list(to) + [(sp, p) for p in peers]:
        pl.semaphore_signal(barrier, inc=1, device_id=target, device_id_type=MESH)
    pl.semaphore_wait(barrier, 2 + n_tp - 1)

    rows, width = res_ref.shape
    per = n // n_tp

    lines = down.shape[2] // CHUNKS

    def own_half(half):
        if narrow:
            return wd_hbm.at[half]
        return wd_hbm.at[:, half * down.shape[3]:(half + 1) * down.shape[3]]

    def d_copy(step, half, c, first):
        span = pl.ds(c * lines, lines)
        if not first:
            src = down.at[step, half, span]
        elif narrow:
            src = wd_hbm.at[half, span]
        else:
            src = wd_hbm.at[span, half * down.shape[3]:(half + 1) * down.shape[3]]
        return pltpu.make_async_remote_copy(
            src_ref=src, dst_ref=down.at[step + 1, half, span],
            send_sem=dsend.at[step, half, c], recv_sem=drecv.at[step, half, c],
            device_id=to[half], device_id_type=MESH,
        )

    def p_copy(k):
        peer = peers[k]
        return pltpu.make_async_remote_copy(
            src_ref=part_ref.at[peer], dst_ref=parts.at[k],
            send_sem=psend.at[k], recv_sem=precv.at[k],
            device_id=(sp, peer), device_id_type=MESH,
        )

    def y_copy(k):
        return pltpu.make_async_remote_copy(
            src_ref=ys.at[tp], dst_ref=ys.at[tp],
            send_sem=ysend.at[k], recv_sem=yrecv.at[k],
            device_id=(sp, peers[k]), device_id_type=MESH,
        )

    def q_copy(k):
        return pltpu.make_async_remote_copy(
            src_ref=sq.at[0], dst_ref=sq.at[k + 1],
            send_sem=qsend.at[k], recv_sem=qrecv.at[k],
            device_id=(sp, peers[k]), device_id_type=MESH,
        )

    def landed(step, c):
        for half in range(2):
            d_copy(step, half, c, True).wait_recv()

    def event(step, c):
        landed(step - 1, c)
        for half in range(2):
            d_copy(step, half, c, False).start()

    def events(first, last):
        for tick in range(first, last):
            event(1 + tick // CHUNKS, tick % CHUNKS)

    for c in range(CHUNKS):
        for half in range(2):
            d_copy(0, half, c, True).start()
    for k in range(n_tp - 1):
        p_copy(k).start()
    loads = [
        pltpu.make_async_copy(
            res_hbm.at[:, pl.ds(pl.multiple_of(tp * width, LANES), width)], res_ref, local.at[0]),
        pltpu.make_async_copy(up_hbm, up, local.at[1]),
        pltpu.make_async_copy(own_half(0), down.at[0, 0], local.at[2]),
        pltpu.make_async_copy(own_half(1), down.at[0, 1], local.at[3]),
    ]
    for load in loads:
        load.start()

    early = 4
    events(0, 6)
    for k in range(n_tp - 1):
        p_copy(k).wait_recv()
    loads[0].wait()
    stream = part_ref[tp].astype(F32)
    for k in range(n_tp - 1):
        stream = stream + parts[k].astype(F32)
    stream = stream + res_ref[...].astype(F32)
    own_stream[...] = stream
    ys[tp] = (stream * gain_ref[tp]).astype(BF16)
    total = jnp.sum(stream * stream, axis=1, keepdims=True)
    sq[0] = jnp.transpose(jnp.broadcast_to(total, (rows, LANES)))[:8]
    for k in range(n_tp - 1):
        q_copy(k).start()
        y_copy(k).start()
    events(6, 12)
    for k in range(n_tp - 1):
        q_copy(k).wait_recv()
    for k in range(n_tp - 1):
        pltpu.make_async_remote_copy(
            src_ref=ys.at[tp], dst_ref=ys.at[(tp + n_tp - 1 - k) % n_tp],
            send_sem=ysend.at[k], recv_sem=yrecv.at[k],
            device_id=(sp, peers[k]), device_id_type=MESH,
        ).wait_recv()
    squares = sq[0]
    for k in range(1, n_tp):
        squares = squares + sq[k]
    squares = jnp.concatenate([squares] * (LANES // 8), axis=0)
    factor = lax.rsqrt(jnp.transpose(squares)[:, :1] / (width * n_tp) + epsilon)
    loads[1].wait()
    units = hidden.shape[1]
    tile = math.gcd(units, 512)

    def up_step(c, carry):
        columns = pl.ds(pl.multiple_of(c * tile, tile), tile)
        total = jnp.dot(ys[0], up[:width, columns], preferred_element_type=F32)
        for t in range(1, n_tp):
            total = total + jnp.dot(
                ys[t], up[t * width:(t + 1) * width, columns], preferred_element_type=F32)
        total = jnp.maximum(total, 0.0) * factor
        hidden[:, columns] = (total * total).astype(BF16)

        @pl.when(c < CHUNKS)
        def _():
            event(early, c)

        return carry

    lax.fori_loop(0, units // tile, up_step, 0)

    def owners(i):
        return at(-i), at(i)

    def f_copy(i, half, owner):
        return pltpu.make_async_remote_copy(
            src_ref=pieces.at[i, half],
            dst_ref=fin.at[tp, owner % per, half],
            send_sem=fsend.at[i, half], recv_sem=frecv.at[tp, owner % per, half],
            device_id=(sp, owner // per), device_id_type=MESH,
        )

    def down_block(i, left, right):
        if narrow:
            block = jnp.concatenate([left, right], axis=0)
            half_width = left.shape[0]
            term = lax.dot_general(hidden[...], block, NT, preferred_element_type=F32)
        else:
            block = jnp.concatenate([left, right], axis=1)
            half_width = left.shape[1]
            term = jnp.dot(hidden[...], block, preferred_element_type=F32)
        term = term.astype(BF16)
        pieces[i, 0] = term[:, :half_width]
        pieces[i, 1] = term[:, half_width:]
        for half, owner in enumerate(owners(i)):

            @pl.when(owner // per != tp)
            def _():
                f_copy(i, half, owner).start()

            @pl.when(owner // per == tp)
            def _():
                fin[tp, owner % per, half] = pieces[i, half]

    for load in loads[2:]:
        load.wait()
    down_block(0, down[0, 0], down[0, 1])

    def down_step(i, carry):
        @pl.when(i <= CHUNKS)
        def _():
            event(early + 1, i - 1)

        @pl.when(i > early + 1)
        def _():
            for c in range(CHUNKS):
                landed(i - 1, c)

                @pl.when(i < n - 1)
                def _():
                    for half in range(2):
                        d_copy(i, half, c, False).start()

        down_block(i, down[i, 0], down[i, 1])
        return carry

    lax.fori_loop(1, n, down_step, 0)

    for k in range(n_tp - 1):
        source = (tp + n_tp - 1 - k) % n_tp
        for o in range(per):
            for half in range(2):
                pltpu.make_async_remote_copy(
                    src_ref=pieces.at[0, half], dst_ref=fin.at[source, o, half],
                    send_sem=fsend.at[0, half], recv_sem=frecv.at[source, o, half],
                    device_id=(sp, peers[k]), device_id_type=MESH,
                ).wait_recv()
    piece = fin.shape[4]
    for o in range(per):
        for half in range(2):
            start = (2 * o + half) * piece
            total = own_stream[:, start:start + piece]
            mixed = fin[0, o, half].astype(F32)
            for t in range(1, n_tp):
                mixed = mixed + fin[t, o, half].astype(F32)
            out_ref[:, start:start + piece] = (total + mixed).astype(BF16)

    def drain(i, carry):
        for c in range(CHUNKS):
            for half in range(2):
                d_copy(i, half, c, True).wait_send()
        return carry

    lax.fori_loop(0, n - 1, drain, 0)

    def drain_pieces(i, carry):
        for half, owner in enumerate(owners(i)):

            @pl.when(owner // per != tp)
            def _():
                f_copy(i, half, owner).wait_send()

        return carry

    lax.fori_loop(0, n, drain_pieces, 0)
    for k in range(n_tp - 1):
        p_copy(k).wait_send()
        q_copy(k).wait_send()
        y_copy(k).wait_send()


def vmem():
    return pl.BlockSpec(memory_space=pltpu.VMEM)


def hbm():
    return pl.BlockSpec(memory_space=pl.ANY)


def on_device(
    n,
    n_tp,
    residual_in,
    queries_nope,
    queries_rope,
    latents,
    rope_keys,
    latent_norm_gain,
    key_up_weight,
    value_up_weight,
    w_out,
    norm_gain,
    w_up,
    w_down,
):
    rows, model = residual_in.shape
    heads = key_up_weight.shape[1] // UNROTATED_WIDTH
    value_width = value_up_weight.shape[1] // heads
    positions = lax.axis_index("sp") * rows + jnp.arange(rows, dtype=jnp.int32)
    phases = rope_phases(positions, ROPE)
    q_rot = rotate(
        queries_rope.astype(F32).reshape(rows, heads, ROPE), phases[:, None, :]
    ).astype(BF16)
    queries = jnp.concatenate(
        [
            queries_nope.reshape(rows, heads, UNROTATED_WIDTH),
            q_rot,
            jnp.zeros((rows, heads, LANES - UNROTATED_WIDTH - ROPE), BF16),
        ],
        axis=2,
    ).reshape(rows, heads * LANES)
    lat_norm = rms_scale(latents.astype(F32), latent_norm_gain).astype(BF16)
    key_rot = rotate(rope_keys.astype(F32), phases).astype(BF16)
    x = jnp.concatenate([lat_norm, key_rot], axis=1)
    wide = x.shape[1]
    x = jnp.transpose(x.reshape(n_tp, rows // n_tp, wide), (0, 2, 1))

    width = model // n_tp
    depth, units = w_up.shape
    dma = pltpu.SemaphoreType.DMA
    part, full = pl.pallas_call(
        functools.partial(
            attention_kernel, n, n_tp, heads,
            math.log2(math.e) / math.sqrt(UNROTATED_WIDTH + ROPE)),
        out_shape=(
            jax.ShapeDtypeStruct((n_tp, rows, width), BF16),
            jax.ShapeDtypeStruct((n, 2, CHUNKS, depth // 2 // CHUNKS, units), BF16),
        ),
        in_specs=[vmem()] * 5 + [hbm()],
        out_specs=(vmem(), hbm()),
        scratch_shapes=[
            pltpu.VMEM(key_up_weight.shape[::-1], BF16),
            pltpu.VMEM(value_up_weight.shape[::-1], BF16),
            pltpu.VMEM((n, n_tp, wide, rows // n_tp), BF16),
            pltpu.VMEM((heads, rows, 1), F32),
            pltpu.VMEM((heads, rows, LANES), F32),
            dma((n - 1,)), dma((n - 1,)),
            dma((n, n_tp - 1)), dma((n, n_tp - 1)),
            dma((n - 1, 2, CHUNKS)), dma((n - 1, 2, CHUNKS)), dma,
        ],
        compiler_params=pltpu.CompilerParams(
            collective_id=0, has_side_effects=True, vmem_limit_bytes=56 * 2**20),
        name="attend",
    )(
        queries, x, key_up_weight, value_up_weight,
        w_out, w_up.reshape(2, CHUNKS, depth // 2 // CHUNKS, units),
    )

    hidden_units, share = w_down.shape
    narrow = (share // 2) % LANES != 0
    if narrow:
        down_in = jnp.transpose(w_down.reshape(hidden_units, 2, share // 2), (1, 2, 0))
        half_shape = (share // 2, hidden_units)
    else:
        down_in = w_down
        half_shape = (hidden_units, share // 2)
    per = n // n_tp
    return pl.pallas_call(
        functools.partial(feed_kernel, n, n_tp, narrow),
        out_shape=jax.ShapeDtypeStruct((rows, width), BF16),
        in_specs=[vmem(), hbm(), vmem(), hbm(), hbm()],
        out_specs=vmem(),
        scratch_shapes=[
            pltpu.VMEM((rows, width), BF16),
            pltpu.VMEM((model, units), BF16),
            pltpu.VMEM((n, 2) + half_shape, BF16),
            pltpu.VMEM((n_tp - 1, rows, width), BF16),
            pltpu.VMEM((n_tp, rows, width), BF16),
            pltpu.VMEM((n_tp, 8, rows), F32),
            pltpu.VMEM((rows, width), F32),
            pltpu.VMEM((rows, units), BF16),
            pltpu.VMEM((n, 2, rows, share // 2), BF16),
            pltpu.VMEM((n_tp, per, 2, rows, share // 2), BF16),
            dma((n - 1, 2, CHUNKS)), dma((n - 1, 2, CHUNKS)),
            dma((n_tp - 1,)), dma((n_tp - 1,)),
            dma((n_tp - 1,)), dma((n_tp - 1,)),
            dma((n_tp - 1,)), dma((n_tp - 1,)),
            dma((n, 2)), dma((n_tp, per, 2)),
            dma((4,)),
        ],
        compiler_params=pltpu.CompilerParams(
            collective_id=1, has_side_effects=True, vmem_limit_bytes=60 * 2**20),
        name="feed",
    )(part, residual_in, norm_gain.reshape(n_tp, 1, width), full.reshape(model, units), down_in)


def solution(mesh):
    in_specs = (
        P("sp", None),
        P("sp", "tp"),
        P("sp", "tp"),
        P("sp", None),
        P("sp", None),
        P(),
        P(None, "tp"),
        P(None, "tp"),
        P("tp", None),
        P(),
        P("sp", "tp"),
        P("tp", "sp"),
    )
    out_specs = P("sp", "tp")
    return jax.shard_map(
        functools.partial(on_device, mesh.shape["sp"], mesh.shape["tp"]),
        mesh=mesh, in_specs=in_specs, out_specs=out_specs, check_vma=False,
    )
```

profile of v0, /device:TPU:0, one launch (start us, length us, event | category | flops | bytes accessed | tf_op | source)
XLA Modules:
  0.0 200.8 jit_solution(16645802762042753335)
XLA Ops:
  0.0 0.0 copy-start
  0.0 0.0 copy-start.1
  0.0 0.1 pad.6.clone
  0.1 1.1 fusion
  1.3 0.8 convert_element_type.22
  2.0 0.2 subtract_convert_fusion.1
  2.2 0.1 copy.20
  2.4 0.1 copy.21
  2.5 1.0 copy.18
  3.6 0.0 copy-done
  3.6 0.8 fusion.2
  4.4 0.1 pad_maximum_fusion
  4.5 0.9 copy.23
  5.5 0.0 copy-done.1
  5.5 0.1 copy.17
  5.6 0.1 maximum_maximum_fusion
  5.8 1.0 copy.24.q_ref
  6.8 99.5 %attend.1 = (bf16[4,512,512]{2,1,0:T(8,128)(2,1)}, bf16[8,2,4,32,2048]{4,3,2,1,0:T(8,128)(2,1)}) custom-call(bf16[512,512]{1,0:T(8,128)(2,1)} %copy.24.q_ref, bf16[4,288,128]{2,1,0:T(8,128)(2,1)} %bitcast.12, bf16[256,256]{1,0:T(8,128)(2,1)} %wk_in.1, bf16[256,256]{1,0:T(8,128)(2,1)} %wv_in.1, bf16[256,2048]{1,0:T(8,128)(2,1)} %wo_ref.1, ...), custom_call_target="tpu_custom_call" | custom-call | tf_op jit(solution)/shard_map/attend/pallas_call | solution.py:498
  106.3 92.6 %feed.1 = bf16[512,512]{1,0:T(8,128)(2,1)} custom-call(bf16[4,512,512]{2,1,0:T(8,128)(2,1)} %get-tuple-element.7.part_ref, bf16[512,2048]{1,0:T(8,128)(2,1)} %res_hbm.1, f32[4,1,512]{2,1,0:T(1,128)} %bitcast.16, bf16[2048,2048]{1,0:T(8,128)(2,1)} %bitcast.9, bf16[2048,256]{1,0:T(8,128)(2,1)} %wd_hbm.1), custom_call_target="tpu_custom_call" | custom-call | tf_op jit(solution)/shard_map/feed/pallas_call | solution.py:535
  198.9 1.9 copy.28
  (6 shorter events, 0.1 us)
Async XLA Ops:
  0.0 3.6 %copy-start = (bf16[512,256]{1,0:T(8,128)(2,1)S(1)}, bf16[512,256]{1,0:T(8,128)(2,1)}, u32[]{:S(2)}) copy-start(bf16[512,256]{1,0:T(8,128)(2,1)} %param.15) | copy-start | bytes 786436
  0.0 5.5 %copy-start.1 = (bf16[512,256]{1,0:T(8,128)(2,1)S(1)}, bf16[512,256]{1,0:T(8,128)(2,1)}, u32[]{:S(2)}) copy-start(bf16[512,256]{1,0:T(8,128)(2,1)} %param.13) | copy-start | bytes 786436
where the time goes:
time: 201 us
  Pallas kernels  192 us (96%)
  local copies, waits for them, and re-layouts  5.28 us (3%)
  other arithmetic  3.27 us (2%)
    pallas_call x1, Pallas kernels, on_device(): pl.pallas_call(functools.partial(attention_kernel, n, n_tp, heads, math.l...  99.5 us
    pallas_call x1, Pallas kernels, on_device(): pl.pallas_call(functools.partial(feed_kernel, n, n_tp, narrow), out_shape...  92.6 us

commit v1 on v0

--- a/solution.py
+++ b/solution.py
@@ -12,6 +12,7 @@
 ROPE = 32
 LANES = 128
 CHUNKS = 4
+CUTS = 2
 
 rope_base = 10000.0
 epsilon = 1e-06
@@ -452,6 +453,612 @@
 
 def hbm():
     return pl.BlockSpec(memory_space=pl.ANY)
+
+
+def fused_kernel(
+    n, n_tp, heads, scale, q_ref, x_ref, wk_in, wv_in, wo_ref, gain_ref, res_hbm, wu, wd,
+    out_ref,
+    wk_ref, wv_ref, xs, keys_ref, vals_ref, peak, acc, res_ref,
+    far32, stream_ref, sbuf, sin, xbuf, xgot, mine, sq_mine, sqs, ys, up, down, hidden,
+    hold, pieces, xin, finh, finz,
+    zx_send, yx_send, x_recv, share_send, share_recv,
+    wz_send, wy_send, wb_send, w_recv, b_recv, own_sem,
+    s_send, s_recv, r_send, r_recv, y_send, y_recv, q_send, q_recv, f_send, f_recv,
+    c_send, c_recv, e_send, e_recv, res_sem,
+):
+    sp = lax.axis_index("sp")
+    tp = lax.axis_index("tp")
+    nz = n // 2
+    z, y = sp // 2, sp % 2
+    x_at, core = tp // 2, tp % 2
+    sib = tp + 1 - 2 * core
+    far = (tp + 2) % n_tp
+    across = sp + 1 - 2 * y
+    mate = 2 * (z + 1 - 2 * (z % 2)) + y
+    turn = 1 - 2 * (z // (nz // 2))
+    peers = [(tp + k) % n_tp for k in range(1, n_tp)]
+
+    def half_of(zz):
+        return ((zz + 1) // 2) % 2
+
+    def z_at(k):
+        return (z + turn * k + nz) % nz
+
+    barrier = pltpu.get_barrier_semaphore()
+    greet = [(2 * ((z + k) % nz) + y, tp) for k in range(1, nz)]
+    greet += [(across, tp)] + [(sp, p) for p in peers] + [(mate, p) for p in peers]
+    for target in greet:
+        pl.semaphore_signal(barrier, inc=1, device_id=target, device_id_type=MESH)
+    pl.semaphore_wait(barrier, len(greet))
+
+    def remote(src, dst, send, recv, target):
+        return pltpu.make_async_remote_copy(
+            src_ref=src, dst_ref=dst, send_sem=send, recv_sem=recv,
+            device_id=target, device_id_type=MESH)
+
+    latent = wk_ref.shape[1]
+    value_width = wv_ref.shape[0] // heads
+    rows = q_ref.shape[0]
+    half = rows // 2
+    width = stream_ref.shape[1]
+    depth = wu.shape[0]
+    units = up.shape[2]
+    cut_u, cut_d = depth // CUTS, units // CUTS
+    share_w = wd.shape[1]
+
+    def span(r):
+        return pl.ds(r * half, half)
+
+    def zx_copy(k):
+        return remote(x_ref.at[tp], xs.at[sp, tp], zx_send.at[k - 1], x_recv.at[sp],
+                      (2 * z_at(k) + y, tp))
+
+    def yx_copy(s, first):
+        return remote(x_ref.at[tp] if first else xs.at[s, tp], xs.at[s, tp],
+                      yx_send.at[s], x_recv.at[s], (across, tp))
+
+    def x_landed(s):
+        remote(x_ref.at[tp], xs.at[s, tp], yx_send.at[s], x_recv.at[s], (across, tp)).wait_recv()
+
+    def share(s, k):
+        return remote(xs.at[s, tp], xs.at[s, tp], share_send.at[s, k], share_recv.at[s, tp],
+                      (sp, peers[k]))
+
+    def share_all(s):
+        for k in range(n_tp - 1):
+            share(s, k).start()
+
+    def share_wait(s):
+        for k in range(n_tp - 1):
+            remote(xs.at[s, tp], xs.at[s, peers[k]], share_send.at[s, k],
+                   share_recv.at[s, peers[k]], (sp, peers[k])).wait_recv()
+
+    def w_src(m, c, h):
+        if m == 0:
+            return wu.at[pl.ds(c * cut_u, cut_u), pl.ds(pl.multiple_of(h * units, LANES), units)]
+        return wd.at[pl.ds(h * units + c * cut_d, cut_d)]
+
+    def w_slot(m, side, s, c):
+        if m == 0:
+            return up.at[side, pl.ds(s * depth + c * cut_u, cut_u)]
+        return down.at[s, pl.ds(side * units + c * cut_d, cut_d)]
+
+    def wz_copy(m, k, c):
+        there = z_at(k)
+        return remote(w_src(m, c, half_of(there)), w_slot(m, core, sp, c),
+                      wz_send.at[m, k - 1, c], w_recv.at[m, sp, c], (2 * there + y, tp))
+
+    def wy_copy(m, s, c, first):
+        slot = w_slot(m, core, s, c)
+        return remote(w_src(m, c, half_of(z)) if first else slot, slot,
+                      wy_send.at[m, s, c], w_recv.at[m, s, c], (across, tp))
+
+    def wb_copy(m, s, c, first):
+        slot = w_slot(m, core, s, c)
+        return remote(w_src(m, c, half_of(z)) if first else slot, slot,
+                      wb_send.at[m, s, c], b_recv.at[m, s, c], (sp, sib))
+
+    def w_landed(m, s, c):
+        slot = w_slot(m, core, s, c)
+        remote(slot, slot, wy_send.at[m, s, c], w_recv.at[m, s, c], (across, tp)).wait_recv()
+
+    def b_landed(m, s):
+        for c in range(CUTS):
+            slot = w_slot(m, 1 - core, s, c)
+            remote(slot, slot, wb_send.at[m, s, c], b_recv.at[m, s, c], (sp, sib)).wait_recv()
+
+    def own_copy(m):
+        h = half_of(z)
+        if m == 0:
+            src = wu.at[:, pl.ds(pl.multiple_of(h * units, LANES), units)]
+            dst = up.at[core, pl.ds(sp * depth, depth)]
+        else:
+            src = wd.at[pl.ds(h * units, units)]
+            dst = down.at[sp, pl.ds(core * units, units)]
+        return pltpu.make_async_copy(src, dst, own_sem.at[m])
+
+    def z_send(m, k):
+        for c in range(CUTS):
+            wz_copy(m, k, c).start()
+
+    def step_of(i):
+        return jnp.where(i == 0, 1, nz - i) if not isinstance(i, int) else (1 if i == 0 else nz - i)
+
+    def from_z(m, i):
+        s = 2 * z_at(step_of(i)) + y
+        for c in range(CUTS):
+            w_landed(m, s, c)
+            wy_copy(m, s, c, False).start()
+            wb_copy(m, s, c, False).start()
+
+    def from_y(m, s):
+        for c in range(CUTS):
+            w_landed(m, s, c)
+            wb_copy(m, s, c, False).start()
+
+    def y_origin(i):
+        return 2 * z_at(step_of(i)) + 1 - y
+
+    for k in range(1, nz):
+        zx_copy(k).start()
+    yx_copy(sp, True).start()
+    for k in [nz - 1] + list(range(1, nz - 1)):
+        z_send(0, k)
+    for m in range(2):
+        own_copy(m).start()
+    for m in range(2):
+        for c in range(CUTS):
+            wb_copy(m, sp, c, True).start()
+    res_copy = pltpu.make_async_copy(
+        res_hbm.at[:, pl.ds(pl.multiple_of(tp * width, LANES), width)], res_ref, res_sem)
+    res_copy.start()
+    wk_ref[...] = jnp.transpose(wk_in[...].astype(F32)).astype(BF16)
+    wv_ref[...] = jnp.transpose(wv_in[...].astype(F32)).astype(BF16)
+    peak[...] = jnp.full(peak.shape, -1e30, F32)
+    acc[...] = jnp.zeros(acc.shape, F32)
+    for t in range(n_tp):
+        xs[sp, t] = x_ref[t]
+
+    def project_keys(s):
+        block = jnp.concatenate([xs[s, t] for t in range(n_tp)], axis=1)
+        lat = block[:latent]
+        rot = block[latent:]
+        count = block.shape[1]
+        k_all = jnp.dot(wk_ref[...], lat, preferred_element_type=F32).astype(BF16)
+        v_all = jnp.dot(wv_ref[...], lat, preferred_element_type=F32).astype(BF16)
+        k_pad = jnp.zeros((LANES - UNROTATED_WIDTH - rot.shape[0], count), BF16)
+        ones = jnp.ones((16, count), BF16)
+        v_pad = jnp.zeros((LANES - value_width - 16, count), BF16)
+        for h in range(heads):
+            keys_ref[s, h] = jnp.concatenate(
+                [k_all[h * UNROTATED_WIDTH:(h + 1) * UNROTATED_WIDTH], rot, k_pad], axis=0)
+            vals_ref[s, h] = jnp.concatenate(
+                [v_all[h * value_width:(h + 1) * value_width], ones, v_pad], axis=0)
+
+    def attend(s, r, size):
+        lines = pl.ds(r * half, size)
+        for h in range(heads):
+            score = jnp.dot(q_ref[lines, h * LANES:(h + 1) * LANES], keys_ref[s, h],
+                            preferred_element_type=F32)
+            old = peak[h, lines]
+            new = jnp.maximum(old, jnp.max(score, axis=1, keepdims=True))
+            p = jnp.exp2((score - new) * scale).astype(BF16)
+            acc[h, lines] = acc[h, lines] * jnp.exp2((old - new) * scale) + lax.dot_general(
+                p, vals_ref[s, h], NT, preferred_element_type=F32)
+            peak[h, lines] = new
+
+    def block_at(b):
+        flip = (b - 2) // (nz - 1)
+        off = (b - 2) % (nz - 1) + 1
+        there = 2 * ((z + off) % nz) + (y + flip) % 2
+        return there
+
+    def s_copy(r):
+        return remote(sbuf.at[r], sin.at[r], s_send.at[r], s_recv.at[r], (sp, sib))
+
+    def r_copy(r):
+        return remote(xbuf.at[r], xgot.at[r], r_send.at[r], r_recv.at[r], (sp, far))
+
+    def project(r):
+        group = []
+        for h in range(heads):
+            a = acc[h, span(r)]
+            group.append((a[:, :value_width] / a[:, value_width:value_width + 1]).astype(BF16))
+        attended = jnp.concatenate(group, axis=1)
+
+        def quarter(t):
+            return jnp.dot(attended, wo_ref[:, pl.ds(pl.multiple_of(t * width, LANES), width)],
+                           preferred_element_type=F32)
+
+        sbuf[r, 0] = quarter(sib).astype(BF16)
+        sbuf[r, 1] = quarter((sib + 2) % n_tp).astype(BF16)
+        s_copy(r).start()
+        far32[span(r)] = quarter(far)
+        stream_ref[span(r)] = quarter(tp)
+
+    def relay(r):
+        s_copy(r).wait_recv()
+        xbuf[r] = (far32[span(r)] + sin[r, 1].astype(F32)).astype(BF16)
+        r_copy(r).start()
+
+    home_far = 2 * (1 - x_at)
+
+    def columns(t):
+        return pl.ds(pl.multiple_of(t * width, LANES), width)
+
+    def y_copy(r, which):
+        target = ((sp, sib), (sp, home_far), (mate, 2 * x_at + 1))[which]
+        return remote(mine.at[span(r)], ys.at[span(r), columns(tp)],
+                      y_send.at[r, which], y_recv.at[r, tp], target)
+
+    def q_copy(r, which):
+        target = ((sp, sib), (sp, home_far), (mate, 2 * x_at + 1), (mate, home_far + 1))[which]
+        return remote(sq_mine.at[r], sqs.at[r, tp], q_send.at[r, which], q_recv.at[r, tp], target)
+
+    def f_copy(r, i):
+        t = 2 * x_at + i
+        return remote(ys.at[span(r), columns(t)], ys.at[span(r), columns(t)],
+                      f_send.at[r, i], y_recv.at[r, t], (sp, home_far + 1))
+
+    def y_wait(r, t):
+        remote(mine.at[span(r)], ys.at[span(r), columns(t)],
+               y_send.at[r, 1], y_recv.at[r, t], (sp, home_far)).wait_recv()
+
+    def q_wait(r, t):
+        remote(sq_mine.at[r], sqs.at[r, t], q_send.at[r, 1], q_recv.at[r, t],
+               (sp, home_far)).wait_recv()
+
+    def settle(r):
+        r_copy(r).wait_recv()
+        stream = stream_ref[span(r)] + sin[r, 0].astype(F32) + xgot[r].astype(F32)
+        stream = stream + res_ref[span(r)].astype(F32)
+        stream_ref[span(r)] = stream
+        shard = (stream * gain_ref[tp]).astype(BF16)
+        mine[span(r)] = shard
+        total = jnp.sum(stream * stream, axis=1, keepdims=True)
+        squares = jnp.transpose(jnp.broadcast_to(total, (half, LANES)))[:8]
+        sq_mine[r] = squares
+
+        @pl.when(core == 0)
+        def _():
+            ys[span(r), columns(tp)] = shard
+            sqs[r, tp] = squares
+
+        q_copy(r, 2).start()
+        y_copy(r, 2).start()
+        q_copy(r, 3).start()
+        q_copy(r, 1).start()
+        y_copy(r, 1).start()
+
+        @pl.when(core == 1)
+        def _():
+            q_copy(r, 0).start()
+            y_copy(r, 0).start()
+
+    def pass_on(r):
+        @pl.when(core == 1)
+        def _():
+            for i in range(2):
+                y_wait(r, 2 * x_at + i)
+                f_copy(r, i).start()
+
+    def gathered(r):
+        @pl.when(core == 1)
+        def _():
+            for i in range(2):
+                y_wait(r, home_far + i)
+            for t in range(n_tp):
+                q_wait(r, t)
+
+        @pl.when(core == 0)
+        def _():
+            for t in peers:
+                y_wait(r, t)
+                q_wait(r, t)
+
+    project_keys(sp)
+    attend(sp, 0, half)
+    x_landed(across)
+    share_all(across)
+    attend(sp, 1, half)
+    for off in range(1, nz):
+        s = 2 * ((z + off) % nz) + y
+        x_landed(s)
+        yx_copy(s, False).start()
+        share_all(s)
+    for m in range(2):
+        for c in range(CUTS):
+            wy_copy(m, sp, c, True).start()
+
+    split = n // 2
+
+    def first_blocks(b, carry):
+        s = jnp.where(b == 1, across, block_at(b))
+        share_wait(s)
+        project_keys(s)
+        attend(s, 0, rows)
+
+        @pl.when(b == 1)
+        def _():
+            for off in range(1, nz):
+                there = 2 * ((z + off) % nz) + 1 - y
+                x_landed(there)
+                share_all(there)
+
+        return carry
+
+    def second_blocks(b, carry):
+        s = block_at(b)
+        share_wait(s)
+        project_keys(s)
+        attend(s, 0, half)
+
+        @pl.when(b == split + 1)
+        def _():
+            from_z(0, 0)
+
+        @pl.when(b == n - 1)
+        def _():
+            from_z(0, 1)
+
+        return carry
+
+    def third_blocks(b, carry):
+        attend(block_at(b), 1, half)
+
+        @pl.when(b == split)
+        def _():
+            relay(0)
+            from_y(0, across)
+
+        @pl.when(b == split + 2)
+        def _():
+            settle(0)
+            z_send(1, 1)
+
+        @pl.when(b == n - 1)
+        def _():
+            from_y(0, y_origin(0))
+
+        return carry
+
+    lax.fori_loop(1, split, first_blocks, 0)
+    lax.fori_loop(split, n, second_blocks, 0)
+    res_copy.wait()
+    project(0)
+    lax.fori_loop(split, n, third_blocks, 0)
+    project(1)
+    relay(1)
+    pass_on(0)
+    settle(1)
+    for k in [nz - 1] + list(range(2, nz - 1)):
+        z_send(1, k)
+    for i in range(2, nz - 1):
+        from_z(0, i)
+    pass_on(1)
+    for i in range(1, nz - 1):
+        from_y(0, y_origin(i))
+    from_z(1, 0)
+    own_copy(0).wait()
+    for s in range(n):
+        b_landed(0, s)
+    gathered(0)
+    gathered(1)
+
+    factors = []
+    for r in range(2):
+        squares = sqs[r, 0]
+        for t in range(1, n_tp):
+            squares = squares + sqs[r, t]
+        squares = jnp.concatenate([squares] * (LANES // 8), axis=0)
+        factors.append(jnp.transpose(squares)[:, :1])
+    factor = lax.rsqrt(jnp.concatenate(factors, axis=0) / (width * n_tp) + epsilon)
+    tile = math.gcd(units, 512)
+    tiles = units // tile
+
+    def up_step(i, carry):
+        within = pl.ds(pl.multiple_of((i % tiles) * tile, tile), tile)
+        total = jnp.dot(ys[...], up[i // tiles, :, within], preferred_element_type=F32)
+        total = jnp.maximum(total, 0.0) * factor
+        hidden[:, pl.ds(pl.multiple_of(i * tile, tile), tile)] = (total * total).astype(BF16)
+        return carry
+
+    lax.fori_loop(0, 2 * tiles, up_step, 0)
+
+    per = n // n_tp
+
+    def order(j):
+        i = (j - 2) // 2
+        there = 2 * z_at(step_of(i)) + (y + j) % 2
+        return jnp.where(j == 0, sp, jnp.where(j == 1, across, there))
+
+    def c_copy(s):
+        return remote(pieces.at[s], xin.at[s % nz], c_send.at[s], c_recv.at[s % nz], (sp, far))
+
+    def e_copy(s):
+        return remote(pieces.at[s], finh.at[s % per], e_send.at[s], e_recv.at[0, s % per],
+                      (sp, s // per))
+
+    def g_copy(s):
+        return remote(pieces.at[s], finz.at[s % per], e_send.at[s], e_recv.at[1, s % per],
+                      (mate, s // per))
+
+    def owner_is_here(s):
+        return s // nz == x_at
+
+    def finish(s):
+        @pl.when(owner_is_here(s))
+        def _():
+            c_copy(s).wait_recv()
+            value = (hold[s % nz] + xin[s % nz].astype(F32)).astype(BF16)
+
+            @pl.when(core == 1)
+            def _():
+                pieces[s] = value
+                g_copy(s).start()
+
+            @pl.when(core == 0)
+            def _():
+                @pl.when(s // per == tp)
+                def _():
+                    finh[s % per] = value
+
+                @pl.when(s // per != tp)
+                def _():
+                    pieces[s] = value
+                    e_copy(s).start()
+
+    own_copy(1).wait()
+
+    def down_step(j, carry):
+        s = order(j)
+        i = (j - 2) // 2
+
+        @pl.when(j % 2 == 1)
+        def _():
+            from_y(1, s)
+
+        @pl.when((j % 2 == 0) & (j >= 4))
+        def _():
+            from_z(1, i)
+
+        b_landed(1, s)
+        term = jnp.dot(hidden[...], down[s], preferred_element_type=F32)
+
+        @pl.when(owner_is_here(s))
+        def _():
+            hold[s % nz] = term
+
+        @pl.when(s // nz != x_at)
+        def _():
+            pieces[s] = term.astype(BF16)
+            c_copy(s).start()
+
+        @pl.when(j > 0)
+        def _():
+            finish(order(j - 1))
+
+        return carry
+
+    lax.fori_loop(0, n, down_step, 0)
+    finish(order(n - 1))
+
+    for o in range(per):
+        s = tp * per + o
+        g_copy(s).wait_recv()
+
+        @pl.when(core == 1)
+        def _():
+            e_copy(s).wait_recv()
+
+        cols = slice(o * share_w, (o + 1) * share_w)
+        out_ref[:, cols] = (
+            stream_ref[:, cols] + (finh[o].astype(F32) + finz[o].astype(F32))).astype(BF16)
+
+    for k in range(1, nz):
+        zx_copy(k).wait_send()
+        for m in range(2):
+            for c in range(CUTS):
+                wz_copy(m, k, c).wait_send()
+    yx_copy(sp, True).wait_send()
+    for k in range(n_tp - 1):
+        share(across, k).wait_send()
+    for off in range(1, nz):
+        s = 2 * ((z + off) % nz) + y
+        yx_copy(s, False).wait_send()
+        for k in range(n_tp - 1):
+            share(s, k).wait_send()
+            share(2 * ((z + off) % nz) + 1 - y, k).wait_send()
+    for off in range(nz):
+        s = 2 * ((z + off) % nz) + y
+        for m in range(2):
+            for c in range(CUTS):
+                wy_copy(m, s, c, False).wait_send()
+
+    def drain(s, carry):
+        for m in range(2):
+            for c in range(CUTS):
+                wb_copy(m, s, c, False).wait_send()
+
+        @pl.when(s // nz != x_at)
+        def _():
+            c_copy(s).wait_send()
+
+        @pl.when(owner_is_here(s) & ((core == 1) | (s // per != tp)))
+        def _():
+            g_copy(s).wait_send()
+
+        return carry
+
+    lax.fori_loop(0, n, drain, 0)
+    for r in range(2):
+        s_copy(r).wait_send()
+        r_copy(r).wait_send()
+        for which in range(1, 3):
+            y_copy(r, which).wait_send()
+        for which in range(1, 4):
+            q_copy(r, which).wait_send()
+
+        @pl.when(core == 1)
+        def _():
+            y_copy(r, 0).wait_send()
+            q_copy(r, 0).wait_send()
+            for i in range(2):
+                f_copy(r, i).wait_send()
+
+
+def fused(n, n_tp, heads, scale, queries, x, key_up, value_up, w_out, gain, residual, w_up, w_down):
+    rows, model = residual.shape
+    depth, units = w_up.shape[0], w_up.shape[1] // 2
+    share_w = w_down.shape[1]
+    width = model // n_tp
+    wide = x.shape[1]
+    half, nz, per = rows // 2, n // 2, n // n_tp
+    dma = pltpu.SemaphoreType.DMA
+    return pl.pallas_call(
+        functools.partial(fused_kernel, n, n_tp, heads, scale),
+        out_shape=jax.ShapeDtypeStruct((rows, width), BF16),
+        in_specs=[vmem()] * 6 + [hbm()] * 3,
+        out_specs=vmem(),
+        scratch_shapes=[
+            pltpu.VMEM(key_up.shape[::-1], BF16),
+            pltpu.VMEM(value_up.shape[::-1], BF16),
+            pltpu.VMEM((n, n_tp, wide, rows // n_tp), BF16),
+            pltpu.VMEM((n, heads, LANES, rows), BF16),
+            pltpu.VMEM((n, heads, LANES, rows), BF16),
+            pltpu.VMEM((heads, rows, 1), F32),
+            pltpu.VMEM((heads, rows, LANES), F32),
+            pltpu.VMEM((rows, width), BF16),
+            pltpu.VMEM((rows, width), F32),
+            pltpu.VMEM((rows, width), F32),
+            pltpu.VMEM((2, 2, half, width), BF16),
+            pltpu.VMEM((2, 2, half, width), BF16),
+            pltpu.VMEM((2, half, width), BF16),
+            pltpu.VMEM((2, half, width), BF16),
+            pltpu.VMEM((rows, width), BF16),
+            pltpu.VMEM((2, 8, half), F32),
+            pltpu.VMEM((2, n_tp, 8, half), F32),
+            pltpu.VMEM((rows, model), BF16),
+            pltpu.VMEM((2, model, units), BF16),
+            pltpu.VMEM((n, 2 * units, share_w), BF16),
+            pltpu.VMEM((rows, 2 * units), BF16),
+            pltpu.VMEM((nz, rows, share_w), F32),
+            pltpu.VMEM((n, rows, share_w), BF16),
+            pltpu.VMEM((nz, rows, share_w), BF16),
+            pltpu.VMEM((per, rows, share_w), BF16),
+            pltpu.VMEM((per, rows, share_w), BF16),
+            dma((nz - 1,)), dma((n,)), dma((n,)), dma((n, n_tp - 1)), dma((n, n_tp)),
+            dma((2, nz - 1, CUTS)), dma((2, n, CUTS)), dma((2, n, CUTS)),
+            dma((2, n, CUTS)), dma((2, n, CUTS)), dma((2,)),
+            dma((2,)), dma((2,)), dma((2,)), dma((2,)),
+            dma((2, 3)), dma((2, n_tp)), dma((2, 4)), dma((2, n_tp)),
+            dma((2, 2)), dma((2, 2)),
+            dma((n,)), dma((nz,)), dma((n,)), dma((2, per)), dma,
+        ],
+        compiler_params=pltpu.CompilerParams(
+            collective_id=2, has_side_effects=True, vmem_limit_bytes=62 * 2**20),
+        name="layer",
+    )(queries, x, key_up, value_up, w_out, gain, residual, w_up, w_down)
 
 
 def on_device(
@@ -494,6 +1101,12 @@
 
     width = model // n_tp
     depth, units = w_up.shape
+    scale = math.log2(math.e) / math.sqrt(UNROTATED_WIDTH + ROPE)
+    lined = depth % (16 * CUTS) == 0 and w_down.shape[1] % LANES == 0 and rows % 256 == 0
+    if n % 4 == 0 and n > 4 and n_tp == 4 and n % (2 * n_tp) == 0 and lined:
+        return fused(
+            n, n_tp, heads, scale, queries, x, key_up_weight, value_up_weight, w_out,
+            norm_gain.reshape(n_tp, 1, width), residual_in, w_up, w_down)
     dma = pltpu.SemaphoreType.DMA
     part, full = pl.pallas_call(
         functools.partial(

time: 201 us -> 191 us (0.950)
  the two profiles are of different devices: /device:TPU:0 before, /device:TPU:6 now
where the time goes in v1:
time: 191 us; the launch traced here: 188 us
  Pallas kernels  179 us (94%)
  local copies, waits for them, and re-layouts  5.24 us (3%)
  other arithmetic  3.27 us (2%)
    pallas_call x1, Pallas kernels, fused(): pl.pallas_call(functools.partial(fused_kernel, n, n_tp, heads, scale), ou...  179 us

profile of v1, /device:TPU:6, one launch (start us, length us, event | category | flops | bytes accessed | tf_op | source)
XLA Modules:
  0.0 187.8 jit_solution(13173410747616445672)
XLA Ops:
  0.0 0.0 copy-start
  0.0 0.0 copy-start.1
  0.0 0.1 pad.6.clone
  0.1 1.1 fusion
  1.3 0.8 convert_element_type.22
  2.0 0.2 subtract_convert_fusion.1
  2.2 0.1 copy.20
  2.4 0.1 copy.21
  2.5 1.0 copy.18
  3.6 0.0 copy-done
  3.6 0.8 fusion.2
  4.4 0.1 pad_maximum_fusion
  4.5 0.9 copy.23
  5.4 0.0 copy-done.1
  5.4 0.1 copy.17
  5.6 0.1 maximum_maximum_fusion
  5.7 1.0 copy.24.q_ref
  6.7 179.2 %layer.1 = bf16[512,512]{1,0:T(8,128)(2,1)} custom-call(bf16[512,512]{1,0:T(8,128)(2,1)} %copy.24.q_ref, bf16[4,288,128]{2,1,0:T(8,128)(2,1)} %bitcast.9, bf16[256,256]{1,0:T(8,128)(2,1)} %wk_in.1, bf16[256,256]{1,0:T(8,128)(2,1)} %wv_in.1, bf16[256,2048]{1,0:T(8,128)(2,1)} %wo_ref.1, f32[4,1,512]{2,1,0:T(1,128)} %bitcast.12, bf16[512,2048]{1,0:T(8,128)(2,1)} %res_hbm.1, ...), custom_call_target="tpu_custom_call" | custom-call | tf_op jit(solution)/shard_map/layer/pallas_call | solution.py:1018
  185.9 1.9 copy.28
  (6 shorter events, 0.1 us)
Async XLA Ops:
  0.0 3.6 %copy-start = (bf16[512,256]{1,0:T(8,128)(2,1)S(1)}, bf16[512,256]{1,0:T(8,128)(2,1)}, u32[]{:S(2)}) copy-start(bf16[512,256]{1,0:T(8,128)(2,1)} %param.15) | copy-start | bytes 786436
  0.0 5.4 %copy-start.1 = (bf16[512,256]{1,0:T(8,128)(2,1)S(1)}, bf16[512,256]{1,0:T(8,128)(2,1)}, u32[]{:S(2)}) copy-start(bf16[512,256]{1,0:T(8,128)(2,1)} %param.13) | copy-start | bytes 786436

commit v2 on v1

--- a/solution.py
+++ b/solution.py
@@ -3,6 +3,7 @@
 
 import jax
 import jax.numpy as jnp
+import numpy as np
 from jax import lax
 from jax.experimental import pallas as pl
 from jax.experimental.pallas import tpu as pltpu
@@ -13,6 +14,7 @@
 LANES = 128
 CHUNKS = 4
 CUTS = 2
+LAG = 3
 
 rope_base = 10000.0
 epsilon = 1e-06
@@ -456,8 +458,10 @@
 
 
 def fused_kernel(
-    n, n_tp, heads, scale, q_ref, x_ref, wk_in, wv_in, wo_ref, gain_ref, res_hbm, wu, wd,
+    n, n_tp, heads, scale, nope_ref, rope_ref, lat_ref, kr_ref, lat_gain, freq_ref, wk_in, wv_in,
+    wo_ref, gain_ref, res_hbm, wu, wd,
     out_ref,
+    q_ref, spin,
     wk_ref, wv_ref, xs, keys_ref, vals_ref, peak, acc, res_ref,
     far32, stream_ref, sbuf, sin, xbuf, xgot, mine, sq_mine, sqs, ys, up, down, hidden,
     hold, pieces, xin, finh, finz,
@@ -475,7 +479,8 @@
     far = (tp + 2) % n_tp
     across = sp + 1 - 2 * y
     mate = 2 * (z + 1 - 2 * (z % 2)) + y
-    turn = 1 - 2 * (z // (nz // 2))
+    turn = 1 - 2 * (z % 2)
+    inner = (z > 0) & (z < nz - 1)
     peers = [(tp + k) % n_tp for k in range(1, n_tp)]
 
     def half_of(zz):
@@ -498,7 +503,7 @@
 
     latent = wk_ref.shape[1]
     value_width = wv_ref.shape[0] // heads
-    rows = q_ref.shape[0]
+    rows = nope_ref.shape[0]
     half = rows // 2
     width = stream_ref.shape[1]
     depth = wu.shape[0]
@@ -510,15 +515,15 @@
         return pl.ds(r * half, half)
 
     def zx_copy(k):
-        return remote(x_ref.at[tp], xs.at[sp, tp], zx_send.at[k - 1], x_recv.at[sp],
+        return remote(xs.at[sp, tp], xs.at[sp, tp], zx_send.at[k - 1], x_recv.at[sp],
                       (2 * z_at(k) + y, tp))
 
-    def yx_copy(s, first):
-        return remote(x_ref.at[tp] if first else xs.at[s, tp], xs.at[s, tp],
+    def yx_copy(s):
+        return remote(xs.at[s, tp], xs.at[s, tp],
                       yx_send.at[s], x_recv.at[s], (across, tp))
 
     def x_landed(s):
-        remote(x_ref.at[tp], xs.at[s, tp], yx_send.at[s], x_recv.at[s], (across, tp)).wait_recv()
+        remote(xs.at[s, tp], xs.at[s, tp], yx_send.at[s], x_recv.at[s], (across, tp)).wait_recv()
 
     def share(s, k):
         return remote(xs.at[s, tp], xs.at[s, tp], share_send.at[s, k], share_recv.at[s, tp],
@@ -582,7 +587,7 @@
             wz_copy(m, k, c).start()
 
     def step_of(i):
-        return jnp.where(i == 0, 1, nz - i) if not isinstance(i, int) else (1 if i == 0 else nz - i)
+        return i + 1
 
     def from_z(m, i):
         s = 2 * z_at(step_of(i)) + y
@@ -599,11 +604,59 @@
     def y_origin(i):
         return 2 * z_at(step_of(i)) + 1 - y
 
+    def grid_of(shape):
+        return (lax.broadcasted_iota(jnp.int32, shape, 0),
+                lax.broadcasted_iota(jnp.int32, shape, 1))
+
+    def picks(hit):
+        return jnp.where(hit, 1.0, 0.0).astype(BF16)
+
+    turn_half = ROPE // 2
+
+    def turned(u, span_of):
+        i, j = grid_of((span_of, span_of))
+        swap = picks((i // ROPE == j // ROPE) & ((i + turn_half) % ROPE == j % ROPE))
+        other = jnp.dot(u, swap, preferred_element_type=F32)
+        return (u.astype(F32) * spin[0, :, :span_of] + other * spin[1, :, :span_of]).astype(BF16)
+
+    def place(out, plain, rotated):
+        i, j = grid_of((heads * UNROTATED_WIDTH, heads * LANES))
+        first = picks((i // UNROTATED_WIDTH == j // LANES) & (i % UNROTATED_WIDTH == j % LANES))
+        i, j = grid_of((heads * ROPE, heads * LANES))
+        second = picks((i // ROPE == j // LANES) & (i % ROPE + UNROTATED_WIDTH == j % LANES))
+        out[...] = (
+            jnp.dot(plain[...], first, preferred_element_type=F32)
+            + jnp.dot(rotated, second, preferred_element_type=F32)).astype(BF16)
+
+    def flipped(u):
+        i, j = grid_of((u.shape[1], u.shape[1]))
+        return lax.dot_general(picks(i == j), u, NT, preferred_element_type=F32).astype(BF16)
+
+    line, lane = grid_of((rows, LANES))
+    phases = (sp * rows + line).astype(F32) * freq_ref[...]
+    spin[0] = jnp.cos(phases)
+    sine = jnp.sin(phases)
+    spin[1] = jnp.where(lane % ROPE < turn_half, -sine, sine)
+    lat = flipped(rms_scale(lat_ref[...].astype(F32), lat_gain[...]).astype(BF16))
+    rot = flipped(turned(kr_ref[...], ROPE))
+    chunk = rows // n_tp
+    for t in range(n_tp):
+        xs[sp, t, :latent] = lat[:, t * chunk:(t + 1) * chunk]
+        xs[sp, t, latent:] = rot[:, t * chunk:(t + 1) * chunk]
+
     for k in range(1, nz):
         zx_copy(k).start()
-    yx_copy(sp, True).start()
-    for k in [nz - 1] + list(range(1, nz - 1)):
+    yx_copy(sp).start()
+    for k in range(1, nz):
         z_send(0, k)
+
+    @pl.when(inner)
+    def _():
+        for k in range(1, nz):
+            z_send(1, k)
+
+    for c in range(CUTS):
+        wy_copy(0, sp, c, True).start()
     for m in range(2):
         own_copy(m).start()
     for m in range(2):
@@ -616,8 +669,7 @@
     wv_ref[...] = jnp.transpose(wv_in[...].astype(F32)).astype(BF16)
     peak[...] = jnp.full(peak.shape, -1e30, F32)
     acc[...] = jnp.zeros(acc.shape, F32)
-    for t in range(n_tp):
-        xs[sp, t] = x_ref[t]
+    place(q_ref, nope_ref, turned(rope_ref[...], LANES))
 
     def project_keys(s):
         block = jnp.concatenate([xs[s, t] for t in range(n_tp)], axis=1)
@@ -764,11 +816,10 @@
     for off in range(1, nz):
         s = 2 * ((z + off) % nz) + y
         x_landed(s)
-        yx_copy(s, False).start()
+        yx_copy(s).start()
         share_all(s)
-    for m in range(2):
-        for c in range(CUTS):
-            wy_copy(m, sp, c, True).start()
+    for c in range(CUTS):
+        wy_copy(1, sp, c, True).start()
 
     split = n // 2
 
@@ -778,12 +829,13 @@
         project_keys(s)
         attend(s, 0, rows)
 
-        @pl.when(b == 1)
+        @pl.when(b == 2)
         def _():
             for off in range(1, nz):
                 there = 2 * ((z + off) % nz) + 1 - y
                 x_landed(there)
                 share_all(there)
+            from_z(0, 0)
 
         return carry
 
@@ -793,12 +845,9 @@
         project_keys(s)
         attend(s, 0, half)
 
-        @pl.when(b == split + 1)
-        def _():
-            from_z(0, 0)
-
         @pl.when(b == n - 1)
         def _():
+            from_y(0, across)
             from_z(0, 1)
 
         return carry
@@ -809,18 +858,18 @@
         @pl.when(b == split)
         def _():
             relay(0)
-            from_y(0, across)
-
-        @pl.when(b == split + 2)
-        def _():
-            settle(0)
-            z_send(1, 1)
-
-        @pl.when(b == n - 1)
+
+        @pl.when(b == split + 1)
         def _():
             from_y(0, y_origin(0))
 
         return carry
+
+    def late_sends(k, c0, c1):
+        @pl.when(z * (nz - 1 - z) == 0)
+        def _():
+            for c in range(c0, c1):
+                wz_copy(1, k, c).start()
 
     lax.fori_loop(1, split, first_blocks, 0)
     lax.fori_loop(split, n, second_blocks, 0)
@@ -828,15 +877,19 @@
     project(0)
     lax.fori_loop(split, n, third_blocks, 0)
     project(1)
+    settle(0)
+    late_sends(1, 0, CUTS // 2)
     relay(1)
-    pass_on(0)
     settle(1)
-    for k in [nz - 1] + list(range(2, nz - 1)):
-        z_send(1, k)
+    late_sends(1, CUTS // 2, CUTS)
+    for k in range(2, nz):
+        late_sends(k, 0, CUTS)
     for i in range(2, nz - 1):
         from_z(0, i)
+    pass_on(0)
+    from_y(0, y_origin(1))
     pass_on(1)
-    for i in range(1, nz - 1):
+    for i in range(2, nz - 1):
         from_y(0, y_origin(i))
     from_z(1, 0)
     own_copy(0).wait()
@@ -861,6 +914,11 @@
         total = jnp.dot(ys[...], up[i // tiles, :, within], preferred_element_type=F32)
         total = jnp.maximum(total, 0.0) * factor
         hidden[:, pl.ds(pl.multiple_of(i * tile, tile), tile)] = (total * total).astype(BF16)
+
+        @pl.when(i == 1)
+        def _():
+            from_z(1, 1)
+
         return carry
 
     lax.fori_loop(0, 2 * tiles, up_step, 0)
@@ -918,9 +976,9 @@
         def _():
             from_y(1, s)
 
-        @pl.when((j % 2 == 0) & (j >= 4))
-        def _():
-            from_z(1, i)
+        @pl.when((j % 2 == 0) & (j >= 4) & (j < n - 2))
+        def _():
+            from_z(1, i + 1)
 
         b_landed(1, s)
         term = jnp.dot(hidden[...], down[s], preferred_element_type=F32)
@@ -934,14 +992,19 @@
             pieces[s] = term.astype(BF16)
             c_copy(s).start()
 
-        @pl.when(j > 0)
-        def _():
-            finish(order(j - 1))
+        @pl.when(j >= LAG)
+        def _():
+            finish(order(j - LAG))
 
         return carry
 
     lax.fori_loop(0, n, down_step, 0)
-    finish(order(n - 1))
+
+    def last_step(j, carry):
+        finish(order(j))
+        return carry
+
+    lax.fori_loop(n - LAG, n, last_step, 0)
 
     for o in range(per):
         s = tp * per + o
@@ -960,12 +1023,12 @@
         for m in range(2):
             for c in range(CUTS):
                 wz_copy(m, k, c).wait_send()
-    yx_copy(sp, True).wait_send()
+    yx_copy(sp).wait_send()
     for k in range(n_tp - 1):
         share(across, k).wait_send()
     for off in range(1, nz):
         s = 2 * ((z + off) % nz) + y
-        yx_copy(s, False).wait_send()
+        yx_copy(s).wait_send()
         for k in range(n_tp - 1):
             share(s, k).wait_send()
             share(2 * ((z + off) % nz) + 1 - y, k).wait_send()
@@ -1007,20 +1070,28 @@
                 f_copy(r, i).wait_send()
 
 
-def fused(n, n_tp, heads, scale, queries, x, key_up, value_up, w_out, gain, residual, w_up, w_down):
+def fused(
+    n, n_tp, heads, scale, queries, rope_queries, latents, rope_keys, latent_gain,
+    key_up, value_up, w_out, gain, residual, w_up, w_down,
+):
     rows, model = residual.shape
     depth, units = w_up.shape[0], w_up.shape[1] // 2
     share_w = w_down.shape[1]
     width = model // n_tp
-    wide = x.shape[1]
+    wide = latents.shape[1] + ROPE
+    rates = np.arange(0, ROPE, 2, dtype=np.float32) / np.float32(ROPE)
+    rates = np.float32(1.0) / np.float32(rope_base) ** rates
+    rates = np.tile(rates, LANES // rates.shape[0])[None, :]
     half, nz, per = rows // 2, n // 2, n // n_tp
     dma = pltpu.SemaphoreType.DMA
     return pl.pallas_call(
         functools.partial(fused_kernel, n, n_tp, heads, scale),
         out_shape=jax.ShapeDtypeStruct((rows, width), BF16),
-        in_specs=[vmem()] * 6 + [hbm()] * 3,
+        in_specs=[vmem()] * 10 + [hbm()] * 3,
         out_specs=vmem(),
         scratch_shapes=[
+            pltpu.VMEM((rows, heads * LANES), BF16),
+            pltpu.VMEM((2, rows, LANES), F32),
             pltpu.VMEM(key_up.shape[::-1], BF16),
             pltpu.VMEM(value_up.shape[::-1], BF16),
             pltpu.VMEM((n, n_tp, wide, rows // n_tp), BF16),
@@ -1058,7 +1129,10 @@
         compiler_params=pltpu.CompilerParams(
             collective_id=2, has_side_effects=True, vmem_limit_bytes=62 * 2**20),
         name="layer",
-    )(queries, x, key_up, value_up, w_out, gain, residual, w_up, w_down)
+    )(
+        queries, rope_queries, latents, rope_keys, latent_gain[None, :], jnp.asarray(rates),
+        key_up, value_up, w_out, gain, residual, w_up, w_down,
+    )
 
 
 def on_device(
@@ -1080,6 +1154,16 @@
     rows, model = residual_in.shape
     heads = key_up_weight.shape[1] // UNROTATED_WIDTH
     value_width = value_up_weight.shape[1] // heads
+    width = model // n_tp
+    depth, units = w_up.shape
+    scale = math.log2(math.e) / math.sqrt(UNROTATED_WIDTH + ROPE)
+    lined = depth % (16 * CUTS) == 0 and w_down.shape[1] % LANES == 0 and rows % 512 == 0
+    fits = heads * ROPE == LANES and n % 4 == 0 and n > 4 and n % (2 * n_tp) == 0
+    if fits and lined and n_tp == 4:
+        return fused(
+            n, n_tp, heads, scale, queries_nope, queries_rope, latents, rope_keys,
+            latent_norm_gain, key_up_weight, value_up_weight, w_out,
+            norm_gain.reshape(n_tp, 1, width), residual_in, w_up, w_down)
     positions = lax.axis_index("sp") * rows + jnp.arange(rows, dtype=jnp.int32)
     phases = rope_phases(positions, ROPE)
     q_rot = rotate(
@@ -1099,19 +1183,10 @@
     wide = x.shape[1]
     x = jnp.transpose(x.reshape(n_tp, rows // n_tp, wide), (0, 2, 1))
 
-    width = model // n_tp
-    depth, units = w_up.shape
-    scale = math.log2(math.e) / math.sqrt(UNROTATED_WIDTH + ROPE)
-    lined = depth % (16 * CUTS) == 0 and w_down.shape[1] % LANES == 0 and rows % 256 == 0
-    if n % 4 == 0 and n > 4 and n_tp == 4 and n % (2 * n_tp) == 0 and lined:
-        return fused(
-            n, n_tp, heads, scale, queries, x, key_up_weight, value_up_weight, w_out,
-            norm_gain.reshape(n_tp, 1, width), residual_in, w_up, w_down)
     dma = pltpu.SemaphoreType.DMA
     part, full = pl.pallas_call(
         functools.partial(
-            attention_kernel, n, n_tp, heads,
-            math.log2(math.e) / math.sqrt(UNROTATED_WIDTH + ROPE)),
+            attention_kernel, n, n_tp, heads, scale),
         out_shape=(
             jax.ShapeDtypeStruct((n_tp, rows, width), BF16),
             jax.ShapeDtypeStruct((n, 2, CHUNKS, depth // 2 // CHUNKS, units), BF16),

time: 191 us -> 146 us (0.76); the launches traced: 188 us -> 145 us
  Pallas kernels: 179 us -> 142 us
  other arithmetic: 3.27 us -> 0 us
    pallas_call x1, Pallas kernels: 179 us -> 142 us  [fused(): pl.pallas_call(functools.partial(fused_kernel, n, n_tp, heads, scale), ou...]
where the time goes in v2:
time: 146 us; the launch traced here: 145 us
  Pallas kernels  142 us (97%)
  local copies, waits for them, and re-layouts  3.39 us (2%)
    pallas_call x1, Pallas kernels, fused(): pl.pallas_call(functools.partial(fused_kernel, n, n_tp, heads, scale), ou...  142 us
    unnamed x2, local copies, waits for them, and re-layouts  3.39 us

profile of v2, /device:TPU:6, one launch (start us, length us, event | category | flops | bytes accessed | tf_op | source)
XLA Modules:
  0.0 145.4 jit_solution(14382208452311008236)
XLA Ops:
  0.0 1.5 %copy.14.kr_ref = bf16[512,32]{1,0:T(8,128)(2,1)} copy(bf16[512,32]{0,1:T(8,128)(2,1)} %param.17) | data formatting | bytes 65536 | tf_op args[4]
  1.5 142.0 %layer.1 = bf16[512,512]{1,0:T(8,128)(2,1)} custom-call(bf16[512,256]{1,0:T(8,128)(2,1)} %nope_ref.1, bf16[512,128]{1,0:T(8,128)(2,1)} %rope_ref.1, bf16[512,256]{1,0:T(8,128)(2,1)} %lat_ref.1, bf16[512,32]{1,0:T(8,128)(2,1)} %copy.14.kr_ref, f32[1,256]{1,0:T(1,128)} %bitcast.3, f32[1,128]{1,0:T(1,128)} %constant.2.clone.freq_ref, bf16[256,256]{1,0:T(8,128)(2,1)} %wk_in.1, ...), custom_call_target="tpu_custom_call" | custom-call | tf_op jit(solution)/shard_map/layer/pallas_call | solution.py:1087
  143.5 1.9 %copy.16 = bf16[512,512]{1,0:T(8,128)(2,1)} copy(bf16[512,512]{1,0:T(8,128)(2,1)} %layer.1) | data formatting | bytes 1048576

commit v3 on v2

--- a/solution.py
+++ b/solution.py
@@ -14,7 +14,7 @@
 LANES = 128
 CHUNKS = 4
 CUTS = 2
-LAG = 3
+LAG = 5
 
 rope_base = 10000.0
 epsilon = 1e-06
@@ -586,6 +586,12 @@
         for c in range(CUTS):
             wz_copy(m, k, c).start()
 
+    def late_sends(k, c0, c1):
+        @pl.when(z * (nz - 1 - z) == 0)
+        def _():
+            for c in range(c0, c1):
+                wz_copy(1, k, c).start()
+
     def step_of(i):
         return i + 1
 
@@ -632,13 +638,21 @@
         i, j = grid_of((u.shape[1], u.shape[1]))
         return lax.dot_general(picks(i == j), u, NT, preferred_element_type=F32).astype(BF16)
 
+
+    @pl.when(inner)
+    def _():
+        wz_copy(0, 2, 0).start()
+
     line, lane = grid_of((rows, LANES))
     phases = (sp * rows + line).astype(F32) * freq_ref[...]
     spin[0] = jnp.cos(phases)
     sine = jnp.sin(phases)
     spin[1] = jnp.where(lane % ROPE < turn_half, -sine, sine)
     lat = flipped(rms_scale(lat_ref[...].astype(F32), lat_gain[...]).astype(BF16))
-    rot = flipped(turned(kr_ref[...], ROPE))
+    i, j = grid_of((ROPE, ROPE))
+    keys = lax.dot_general(
+        kr_ref[...], picks(i == j), (((0,), (0,)), ((), ())), preferred_element_type=F32)
+    rot = flipped(turned(keys.astype(BF16), ROPE))
     chunk = rows // n_tp
     for t in range(n_tp):
         xs[sp, t, :latent] = lat[:, t * chunk:(t + 1) * chunk]
@@ -647,7 +661,16 @@
     for k in range(1, nz):
         zx_copy(k).start()
     yx_copy(sp).start()
-    for k in range(1, nz):
+    for c in range(0, CUTS):
+        wz_copy(0, 1, c).start()
+
+    @pl.when(z * (nz - 1 - z) == 0)
+    def _():
+        wz_copy(0, 2, 0).start()
+
+    for c in range(1, CUTS):
+        wz_copy(0, 2, c).start()
+    for k in range(3, nz):
         z_send(0, k)
 
     @pl.when(inner)
@@ -655,6 +678,7 @@
         for k in range(1, nz):
             z_send(1, k)
 
+    late_sends(1, 0, CUTS)
     for c in range(CUTS):
         wy_copy(0, sp, c, True).start()
     for m in range(2):
@@ -865,12 +889,6 @@
 
         return carry
 
-    def late_sends(k, c0, c1):
-        @pl.when(z * (nz - 1 - z) == 0)
-        def _():
-            for c in range(c0, c1):
-                wz_copy(1, k, c).start()
-
     lax.fori_loop(1, split, first_blocks, 0)
     lax.fori_loop(split, n, second_blocks, 0)
     res_copy.wait()
@@ -878,14 +896,13 @@
     lax.fori_loop(split, n, third_blocks, 0)
     project(1)
     settle(0)
-    late_sends(1, 0, CUTS // 2)
+    late_sends(2, 0, CUTS // 2)
     relay(1)
-    settle(1)
-    late_sends(1, CUTS // 2, CUTS)
-    for k in range(2, nz):
-        late_sends(k, 0, CUTS)
     for i in range(2, nz - 1):
         from_z(0, i)
+    settle(1)
+    late_sends(2, CUTS // 2, CUTS)
+    late_sends(3, 0, CUTS)
     pass_on(0)
     from_y(0, y_origin(1))
     pass_on(1)
@@ -930,16 +947,17 @@
         there = 2 * z_at(step_of(i)) + (y + j) % 2
         return jnp.where(j == 0, sp, jnp.where(j == 1, across, there))
 
-    def c_copy(s):
-        return remote(pieces.at[s], xin.at[s % nz], c_send.at[s], c_recv.at[s % nz], (sp, far))
-
-    def e_copy(s):
-        return remote(pieces.at[s], finh.at[s % per], e_send.at[s], e_recv.at[0, s % per],
-                      (sp, s // per))
-
-    def g_copy(s):
-        return remote(pieces.at[s], finz.at[s % per], e_send.at[s], e_recv.at[1, s % per],
-                      (mate, s // per))
+    def c_copy(s, r):
+        return remote(pieces.at[s, span(r)], xin.at[s % nz, span(r)], c_send.at[s, r],
+                      c_recv.at[s % nz, r], (sp, far))
+
+    def e_copy(s, r):
+        return remote(pieces.at[s, span(r)], finh.at[s % per, span(r)], e_send.at[s, r],
+                      e_recv.at[0, s % per, r], (sp, s // per))
+
+    def g_copy(s, r):
+        return remote(pieces.at[s, span(r)], finz.at[s % per, span(r)], e_send.at[s, r],
+                      e_recv.at[1, s % per, r], (mate, s // per))
 
     def owner_is_here(s):
         return s // nz == x_at
@@ -947,24 +965,25 @@
     def finish(s):
         @pl.when(owner_is_here(s))
         def _():
-            c_copy(s).wait_recv()
-            value = (hold[s % nz] + xin[s % nz].astype(F32)).astype(BF16)
-
-            @pl.when(core == 1)
-            def _():
-                pieces[s] = value
-                g_copy(s).start()
-
-            @pl.when(core == 0)
-            def _():
-                @pl.when(s // per == tp)
+            for r in range(2):
+                c_copy(s, r).wait_recv()
+                value = (hold[s % nz, span(r)] + xin[s % nz, span(r)].astype(F32)).astype(BF16)
+
+                @pl.when((core == 0) & (s // per == tp))
                 def _():
-                    finh[s % per] = value
-
-                @pl.when(s // per != tp)
+                    finh[s % per, span(r)] = value
+
+                @pl.when((core == 1) | (s // per != tp))
                 def _():
-                    pieces[s] = value
-                    e_copy(s).start()
+                    pieces[s, span(r)] = value
+
+                    @pl.when(core == 1)
+                    def _():
+                        g_copy(s, r).start()
+
+                    @pl.when(core == 0)
+                    def _():
+                        e_copy(s, r).start()
 
     own_copy(1).wait()
 
@@ -990,7 +1009,8 @@
         @pl.when(s // nz != x_at)
         def _():
             pieces[s] = term.astype(BF16)
-            c_copy(s).start()
+            for r in range(2):
+                c_copy(s, r).start()
 
         @pl.when(j >= LAG)
         def _():
@@ -1008,15 +1028,17 @@
 
     for o in range(per):
         s = tp * per + o
-        g_copy(s).wait_recv()
-
-        @pl.when(core == 1)
-        def _():
-            e_copy(s).wait_recv()
-
         cols = slice(o * share_w, (o + 1) * share_w)
-        out_ref[:, cols] = (
-            stream_ref[:, cols] + (finh[o].astype(F32) + finz[o].astype(F32))).astype(BF16)
+        for r in range(2):
+            g_copy(s, r).wait_recv()
+
+            @pl.when(core == 1)
+            def _():
+                e_copy(s, r).wait_recv()
+
+            out_ref[span(r), cols] = (
+                stream_ref[span(r), cols]
+                + (finh[o, span(r)].astype(F32) + finz[o, span(r)].astype(F32))).astype(BF16)
 
     for k in range(1, nz):
         zx_copy(k).wait_send()
@@ -1045,11 +1067,13 @@
 
         @pl.when(s // nz != x_at)
         def _():
-            c_copy(s).wait_send()
+            for r in range(2):
+                c_copy(s, r).wait_send()
 
         @pl.when(owner_is_here(s) & ((core == 1) | (s // per != tp)))
         def _():
-            g_copy(s).wait_send()
+            for r in range(2):
+                g_copy(s, r).wait_send()
 
         return carry
 
@@ -1124,13 +1148,13 @@
             dma((2,)), dma((2,)), dma((2,)), dma((2,)),
             dma((2, 3)), dma((2, n_tp)), dma((2, 4)), dma((2, n_tp)),
             dma((2, 2)), dma((2, 2)),
-            dma((n,)), dma((nz,)), dma((n,)), dma((2, per)), dma,
+            dma((n, 2)), dma((nz, 2)), dma((n, 2)), dma((2, per, 2)), dma,
         ],
         compiler_params=pltpu.CompilerParams(
             collective_id=2, has_side_effects=True, vmem_limit_bytes=62 * 2**20),
         name="layer",
     )(
-        queries, rope_queries, latents, rope_keys, latent_gain[None, :], jnp.asarray(rates),
+        queries, rope_queries, latents, jnp.transpose(rope_keys), latent_gain[None, :], jnp.asarray(rates),
         key_up, value_up, w_out, gain, residual, w_up, w_down,
     )
 

time: 146 us -> 136 us (0.932)
  Pallas kernels: 142 us -> 134 us
  local copies, waits for them, and re-layouts: 3.39 us -> 1.87 us
    pallas_call x1, Pallas kernels: 142 us -> 134 us  [fused(): pl.pallas_call(functools.partial(fused_kernel, n, n_tp, heads, scale), ou...]
    unnamed x2 -> x1, local copies, waits for them, and re-layouts: 3.39 us -> 1.87 us
where the time goes in v3:
time: 136 us
  Pallas kernels  134 us (99%)
  local copies, waits for them, and re-layouts  1.87 us (1%)
    pallas_call x1, Pallas kernels, fused(): pl.pallas_call(functools.partial(fused_kernel, n, n_tp, heads, scale), ou...  134 us

profile of v3, /device:TPU:6, one launch (start us, length us, event | category | flops | bytes accessed | tf_op | source)
XLA Modules:
  0.0 136.1 jit_solution(17178364339281811810)
XLA Ops:
  0.0 134.2 %layer.1 = bf16[512,512]{1,0:T(8,128)(2,1)} custom-call(bf16[512,256]{1,0:T(8,128)(2,1)} %nope_ref.1, bf16[512,128]{1,0:T(8,128)(2,1)} %rope_ref.1, bf16[512,256]{1,0:T(8,128)(2,1)} %lat_ref.1, bf16[32,512]{1,0:T(8,128)(2,1)} %bitcast.3, f32[1,256]{1,0:T(1,128)} %bitcast.5, f32[1,128]{1,0:T(1,128)} %constant.2.clone.freq_ref, bf16[256,256]{1,0:T(8,128)(2,1)} %wk_in.1, ...), custom_call_target="tpu_custom_call" | custom-call | tf_op jit(solution)/shard_map/layer/pallas_call | solution.py:1111
  134.2 1.9 %copy.15 = bf16[512,512]{1,0:T(8,128)(2,1)} copy(bf16[512,512]{1,0:T(8,128)(2,1)} %layer.1) | data formatting | bytes 1048576

commit v4 on v3

--- a/solution.py
+++ b/solution.py
@@ -459,9 +459,9 @@
 
 def fused_kernel(
     n, n_tp, heads, scale, nope_ref, rope_ref, lat_ref, kr_ref, lat_gain, freq_ref, wk_in, wv_in,
-    wo_ref, gain_ref, res_hbm, wu, wd,
+    wo_hbm, gain_ref, res_hbm, wu, wd,
     out_ref,
-    q_ref, spin,
+    wo_ref, wo_sem, q_ref, spin,
     wk_ref, wv_ref, xs, keys_ref, vals_ref, peak, acc, res_ref,
     far32, stream_ref, sbuf, sin, xbuf, xgot, mine, sq_mine, sqs, ys, up, down, hidden,
     hold, pieces, xin, finh, finz,
@@ -689,6 +689,8 @@
     res_copy = pltpu.make_async_copy(
         res_hbm.at[:, pl.ds(pl.multiple_of(tp * width, LANES), width)], res_ref, res_sem)
     res_copy.start()
+    wo_copy = pltpu.make_async_copy(wo_hbm, wo_ref, wo_sem)
+    wo_copy.start()
     wk_ref[...] = jnp.transpose(wk_in[...].astype(F32)).astype(BF16)
     wv_ref[...] = jnp.transpose(wv_in[...].astype(F32)).astype(BF16)
     peak[...] = jnp.full(peak.shape, -1e30, F32)
@@ -892,6 +894,7 @@
     lax.fori_loop(1, split, first_blocks, 0)
     lax.fori_loop(split, n, second_blocks, 0)
     res_copy.wait()
+    wo_copy.wait()
     project(0)
     lax.fori_loop(split, n, third_blocks, 0)
     project(1)
@@ -904,11 +907,10 @@
     late_sends(2, CUTS // 2, CUTS)
     late_sends(3, 0, CUTS)
     pass_on(0)
-    from_y(0, y_origin(1))
-    pass_on(1)
-    for i in range(2, nz - 1):
+    for i in range(1, nz - 1):
         from_y(0, y_origin(i))
     from_z(1, 0)
+    pass_on(1)
     own_copy(0).wait()
     for s in range(n):
         b_landed(0, s)
@@ -1111,9 +1113,10 @@
     return pl.pallas_call(
         functools.partial(fused_kernel, n, n_tp, heads, scale),
         out_shape=jax.ShapeDtypeStruct((rows, width), BF16),
-        in_specs=[vmem()] * 10 + [hbm()] * 3,
+        in_specs=[vmem()] * 8 + [hbm(), vmem()] + [hbm()] * 3,
         out_specs=vmem(),
         scratch_shapes=[
+            pltpu.VMEM(w_out.shape, BF16), dma,
             pltpu.VMEM((rows, heads * LANES), BF16),
             pltpu.VMEM((2, rows, LANES), F32),
             pltpu.VMEM(key_up.shape[::-1], BF16),

time: 136 us -> 136 us (level)
  no operation moved by 1% of the time
where the time goes in v4:
time: 136 us
  Pallas kernels  134 us (99%)
  local copies, waits for them, and re-layouts  1.87 us (1%)
    pallas_call x1, Pallas kernels, fused(): pl.pallas_call(functools.partial(fused_kernel, n, n_tp, heads, scale), ou...  134 us

profile of v4, /device:TPU:6, one launch (start us, length us, event | category | flops | bytes accessed | tf_op | source)
XLA Modules:
  0.0 135.8 jit_solution(16471015290783894077)
XLA Ops:
  0.0 133.9 %layer.1 = bf16[512,512]{1,0:T(8,128)(2,1)} custom-call(bf16[512,256]{1,0:T(8,128)(2,1)} %nope_ref.1, bf16[512,128]{1,0:T(8,128)(2,1)} %rope_ref.1, bf16[512,256]{1,0:T(8,128)(2,1)} %lat_ref.1, bf16[32,512]{1,0:T(8,128)(2,1)} %bitcast.3, f32[1,256]{1,0:T(1,128)} %bitcast.5, f32[1,128]{1,0:T(1,128)} %constant.2.clone.freq_ref, bf16[256,256]{1,0:T(8,128)(2,1)} %wk_in.1, ...), custom_call_target="tpu_custom_call" | custom-call | tf_op jit(solution)/shard_map/layer/pallas_call | solution.py:1113
  133.9 1.9 %copy.15 = bf16[512,512]{1,0:T(8,128)(2,1)} copy(bf16[512,512]{1,0:T(8,128)(2,1)} %layer.1) | data formatting | bytes 1048576
